TPU v7x, 32 devices: a whole 2x2x4 slice. The times are simulated.
32 devices in a mesh: sp: 8 (over z, y), tp: 4 (over x, core).
Axes of the slice: x: 2, y: 2, z: 4, core: 2. Of those that a mesh axis runs over, the one named last changes fastest.
Arguments:
- prompt_input: bfloat16 [2304, 2048], P('sp'), may hold values from -6 to 6
- next_input: bfloat16 [2048], replicated, may hold values from -6 to 6
- norm_gain: float32 [2048], replicated, may hold values from 0.1 to 1.9
- w_key: bfloat16 [2048, 1024], P(None, 'tp'), may hold values from -0.125 to 0.125
- w_value: bfloat16 [2048, 1024], P(None, 'tp'), may hold values from -0.125 to 0.125
- w_query: bfloat16 [2048, 1024], P(None, 'tp'), may hold values from -0.125 to 0.125
- key_offset: float32 [2304, 8], P('sp', 'tp'), may hold values from -10 to 0, as said below
Outputs:
- key_cache: bfloat16 [8, 8, 36, 1024], P('sp', None, None, 'tp')
- value_cache: bfloat16 [8, 8, 36, 1024], P('sp', None, None, 'tp')
- reading: bfloat16 [1024], replicated
Inputs may be any that keep to these rules, and one draw needn't show every extreme that they name: `key_offset`: finite log-odds offsets, one per key and head.
All inputs are finite; a program needn't handle non-finite values.
Results may differ from a plain program's by a relative error of at most 0.011.
Values may be sent and summed in bfloat16 or wider, within the bound.
A program may use at most 64 MiB of HBM per device.

v0:
```python
import jax
import jax.numpy as jnp
from jax import lax
from jax.sharding import PartitionSpec as P

HEAD_DIM = 128


def norm_rows(row_block, gain_vec):
    wide_rows = row_block.astype(jnp.float32)
    inv_rms = lax.rsqrt(jnp.mean(wide_rows * wide_rows, axis=-1, keepdims=True) + 1e-06)
    return (wide_rows * inv_rms * gain_vec).astype(jnp.bfloat16)


def shards(prompt_input, next_input, norm_gain, w_key, w_value, w_query, key_offset):
    span_len = prompt_input.shape[0]
    head_width = w_key.shape[1]
    heads_here = head_width // HEAD_DIM
    score_scale = HEAD_DIM ** (-0.5)
    slots = lax.axis_size("sp")
    sub_len = span_len // slots
    normed = norm_rows(prompt_input, norm_gain)
    key_rows = jnp.dot(normed, w_key, preferred_element_type=jnp.float32).astype(jnp.bfloat16)
    value_rows = jnp.dot(normed, w_value, preferred_element_type=jnp.float32).astype(jnp.bfloat16)
    outgoing = jnp.stack([key_rows, value_rows]).reshape(2, slots, 1, sub_len, head_width)
    arrived = lax.all_to_all(outgoing, "sp", split_axis=1, concat_axis=2, tiled=True)
    key_cache = arrived[0]
    value_cache = arrived[1]
    new_query = jnp.dot(
        norm_rows(next_input[None, :], norm_gain), w_query, preferred_element_type=jnp.float32
    )
    new_query = new_query.astype(jnp.bfloat16).reshape(heads_here, HEAD_DIM)
    key_heads = key_rows.reshape(span_len, heads_here, HEAD_DIM)
    value_heads = value_rows.reshape(span_len, heads_here, HEAD_DIM)
    logits = (
        jnp.einsum("hd,shd->sh", new_query, key_heads, preferred_element_type=jnp.float32)
        * score_scale
        + key_offset
    )
    log_breaks = jax.nn.log_sigmoid(-logits)
    inner_sum = lax.cumsum(log_breaks, axis=0, reverse=True) - log_breaks
    block_totals = jnp.sum(log_breaks, axis=0)
    every_total = lax.all_gather(block_totals[None], "sp", axis=0, tiled=True)
    block_ids = lax.broadcasted_iota(jnp.int32, every_total.shape, 0)
    carried = jnp.sum(jnp.where(block_ids > lax.axis_index("sp"), every_total, 0.0), axis=0)
    weights = jnp.exp(jax.nn.log_sigmoid(logits) + inner_sum + carried[None, :])
    partial_value = jnp.einsum("sh,shd->hd", weights, value_heads.astype(jnp.float32))
    summed = lax.psum(partial_value, "sp")
    own_read = summed.reshape(head_width).astype(jnp.bfloat16)
    reading = lax.all_gather(own_read, "tp", axis=0, tiled=True)
    return (key_cache, value_cache, reading)


def solution(mesh):
    placed = (P("sp", None), P(), P(), P(None, "tp"), P(None, "tp"), P(None, "tp"), P("sp", "tp"))
    return jax.shard_map(
        shards,
        mesh=mesh,
        in_specs=placed,
        out_specs=(P("sp", None, None, "tp"), P("sp", None, None, "tp"), P()),
        check_vma=False,
    )
```

profile of v0, /device:TPU:0, one launch (start us, length us, event | category | flops | bytes accessed | tf_op | source)
XLA Modules:
  0.0 65.4 jit_solution(9334492287471043287)
XLA Ops:
  0.6 0.0 copy-start
  0.7 1.7 %fusion = f32[288]{0:T(512)S(1)} fusion(bf16[288,2048]{1,0:T(8,128)(2,1)} %param.7), kind=kLoop, calls=%fused_computation.2 | loop fusion | flops 1769184 | bytes 1180800 | tf_op jit(solution)/shard_map/reduce_sum | solution.py:11
  2.4 0.2 copy-done.1
  2.6 1.3 %convolution_convert_fusion = bf16[288,256]{1,0:T(8,128)(2,1)S(1)} fusion(bf16[2048,256]{1,0:T(8,128)(2,1)S(1)} %copy-done, bf16[288,2048]{1,0:T(8,128)(2,1)S(1)} %copy-done.1, f32[2048]{0:T(1024)} %param.9, f32[288]{0:T(512)S(1)} %add_rsqrt_fusion), kind=kOutput, calls=%fused_computation.5 | convolution fusion | flops 304422912 | bytes 2385024 | tf_op jit(solution)/shard_map/dot_general | solution.py:24
  3.9 0.5 convolution_convert_fusion.1
  4.5 0.0 copy-start.3
  4.5 0.0 copy-start.2
  4.6 0.0 copy-start.7
  4.6 0.0 copy-start.4
  4.6 1.0 %copy.17 = bf16[2,8,1,36,256]{4,0,3,2,1:T(2,128)(2,1)} copy(bf16[2,8,1,36,256]{4,3,1,2,0:T(8,128)(2,1)S(1)} %pad_maximum_fusion) | data formatting | bytes 589824 | tf_op jit(solution)/shard_map/stack | solution.py:25
  5.6 7.3 %all-to-all-start = ((bf16[2,8,1,36,256]{4,0,3,2,1:T(2,128)(2,1)}), bf16[2,8,1,36,256]{4,0,3,2,1:T(2,128)(2,1)S(1)}, u32[]{:S(2)}, u32[]{:S(2)}) async-start(bf16[2,8,1,36,256]{4,0,3,2,1:T(2,128)(2,1)} %copy.17), calls=%async_computation | async-start | bytes 589824 | tf_op jit(solution)/shard_map/all_to_all | solution.py:26
  13.0 0.6 fusion.11
  14.3 0.2 fusion.21
  14.5 0.1 fusion.8
  14.7 0.6 dynamic-slice
  16.0 0.1 fusion.19
  16.1 0.1 negate_dynamic-update-slice_fusion
  16.2 21.8 %all-reduce.1 = f32[16]{0:T(128)S(1)} all-reduce(f32[16]{0:T(128)S(1)} %negate_dynamic-update-slice_fusion), channel_id=2, replica_groups=mesh['sp'=8,'tp'=4] {'sp'}, use_global_device_ids=true, to_apply=%add.1 | all-reduce | flops 16 | bytes 128
  38.1 2.5 %reduce-window.6 = f32[2,3,128]{2,1,0:T(4,128)S(1)} reduce-window(f32[2,3,128]{2,1,0:T(4,128)S(1)} %reshape.81, f32[]{:T(128)} %constant.20.clone.1), window={size=1x1x128 pad=0_0x0_0x0_127}, to_apply=%region_2.3 | reduce-window | flops 97536 | bytes 6148 | tf_op jit(solution)/shard_map/reduce-window
  40.6 0.1 slice_reduce_fusion
  40.7 0.2 reduce-window.9
  40.9 0.1 slice.21
  40.9 0.1 add_bitcast_fusion
  41.0 0.1 reshape.84
  41.1 0.1 select_reduce_fusion
  41.2 0.1 exponential_bitcast_fusion
  41.3 0.1 fusion.5
  41.4 17.1 %psum.7 = bf16[2,128]{1,0:T(2,128)(2,1)S(1)} all-reduce(f32[2,128]{1,0:T(2,128)S(1)} %bitcast.64), channel_id=1, replica_groups=mesh['sp'=8,'tp'=4] {'sp'}, use_global_device_ids=true, to_apply=%region_6.7 | all-reduce | flops 256 | bytes 1536 | tf_op jit(solution)/shard_map/psum | solution.py:48
  58.6 5.1 %all-gather.1 = bf16[4,1,256]{2,1,0:T(2,128)(2,1)S(1)} all-gather(bf16[1,1,256]{2,1,0:T(2,128)(2,1)S(1)} %reshape.88), channel_id=1, replica_groups=mesh['sp'=8,'tp'=4] {'tp'}, dimensions={0}, use_global_device_ids=true | all-gather | bytes 2560 | tf_op jit(solution)/shard_map/all_gather | solution.py:50
  63.6 0.6 copy.31
  64.2 0.4 fusion.20
  64.6 0.8 %copy_bitcast_fusion = (bf16[1,8,36,256]{3,1,2,0:T(8,128)(2,1)}, bf16[1,8,36,256]{3,1,2,0:T(8,128)(2,1)}) fusion(bf16[1,8,1,36,256]{4,0,3,2,1:T(2,128)(2,1)S(1)} %get-tuple-element.11, bf16[1,8,1,36,256]{4,0,3,2,1:T(2,128)(2,1)S(1)} %get-tuple-element.12), kind=kLoop, calls=%fused_computation.14 | loop fusion | bytes 589824 | tf_op jit(solution)/shard_map/squeeze | solution.py:28
  (26 shorter events, 0.2 us)
Async XLA Ops:
  0.6 1.8 %copy-start = (bf16[2048,256]{1,0:T(8,128)(2,1)S(1)}, bf16[2048,256]{1,0:T(8,128)(2,1)}, u32[]{:S(2)}) copy-start(bf16[2048,256]{1,0:T(8,128)(2,1)} %param.11) | copy-start | bytes 3145732
  0.6 1.9 %copy-start.1 = (bf16[288,2048]{1,0:T(8,128)(2,1)S(1)}, bf16[288,2048]{1,0:T(8,128)(2,1)}, u32[]{:S(2)}) copy-start(bf16[288,2048]{1,0:T(8,128)(2,1)} %param.7) | copy-start | bytes 3538948
  2.6 1.3 %copy-start.5 = (f32[2048]{0:T(1024)S(1)}, f32[2048]{0:T(1024)}, u32[]{:S(2)}) copy-start(f32[2048]{0:T(1024)} %param.9) | copy-start | bytes 24580
  2.6 1.3 %copy-start.6 = (bf16[2048,256]{1,0:T(8,128)(2,1)S(1)}, bf16[2048,256]{1,0:T(8,128)(2,1)}, u32[]{:S(2)}) copy-start(bf16[2048,256]{1,0:T(8,128)(2,1)} %param.10) | copy-start | bytes 3145732
  4.5 8.5 %copy-start.3 = (bf16[2048]{0:T(1024)(128)(2,1)S(1)}, bf16[2048]{0:T(1024)(128)(2,1)}, u32[]{:S(2)}) copy-start(bf16[2048]{0:T(1024)(128)(2,1)} %param.8) | copy-start | bytes 12292
  4.5 9.8 %copy-start.2 = (bf16[2048,256]{1,0:T(8,128)(2,1)S(1)}, bf16[2048,256]{1,0:T(8,128)(2,1)}, u32[]{:S(2)}) copy-start(bf16[2048,256]{1,0:T(8,128)(2,1)} %param.12) | copy-start | bytes 3145732
  4.6 10.1 %copy-start.7 = (u32[32]{0:T(128)S(1)}, u32[32]{0:T(128)}, u32[]{:S(2)}) copy-start(u32[32]{0:T(128)} %constant.31) | copy-start | bytes 388
  4.6 11.3 %copy-start.4 = (f32[288,2]{0,1:T(2,128)S(1)}, f32[288,2]{0,1:T(2,128)}, u32[]{:S(2)}) copy-start(f32[288,2]{0,1:T(2,128)} %param.13) | copy-start | bytes 6916
  5.6 58.6 %all-to-all-start = ((bf16[2,8,1,36,256]{4,0,3,2,1:T(2,128)(2,1)}), bf16[2,8,1,36,256]{4,0,3,2,1:T(2,128)(2,1)S(1)}, u32[]{:S(2)}, u32[]{:S(2)}) async-start(bf16[2,8,1,36,256]{4,0,3,2,1:T(2,128)(2,1)} %copy.17), calls=%async_computation | async-start | bytes 589824 | tf_op jit(solution)/shard_map/all_to_all | solution.py:26
where the time goes:
time: 65.7 us; the launch traced here: 65.4 us
  blocking collectives  44 us (67%)
  starting transfers between devices  7.31 us (11%)
  other arithmetic  5.61 us (9%)
  local copies, waits for them, and re-layouts  3.98 us (6%)
  matrix products  2.36 us (4%)
  between operations  2.15 us (3%)
    unnamed x1, blocking collectives  21.8 us
    psum x1, blocking collectives, shards(): summed = lax.psum(partial_value, 'sp')  17.1 us
    all_to_all x1, starting transfers between devices, shards(): lax.all_to_all(outgoing, 'sp', split_axis=1, concat_axis=2, tiled=True)  7.31 us
    all_gather x1, blocking collectives, shards(): reading = lax.all_gather(own_read, 'tp', axis=0, tiled=True)  5.05 us
    another operation x2, other arithmetic  2.71 us
    reduce_sum x2, other arithmetic, norm_rows(): jnp.mean(wide_rows * wide_rows, axis=-1, keepdims=True) + 1e-06  2.34 us
    unnamed x21, local copies, waits for them, and re-layouts  1.43 us
  transfers between devices with their start and end apart: 1, of which 0 were waited for; matrix products, arithmetic and copies ran while one was open for 9% of the time, Pallas kernels for 0%

commit v1 on v0

--- a/solution.py
+++ b/solution.py
@@ -45,7 +45,9 @@
     carried = jnp.sum(jnp.where(block_ids > lax.axis_index("sp"), every_total, 0.0), axis=0)
     weights = jnp.exp(jax.nn.log_sigmoid(logits) + inner_sum + carried[None, :])
     partial_value = jnp.einsum("sh,shd->hd", weights, value_heads.astype(jnp.float32))
-    summed = lax.psum(partial_value, "sp")
+    summed = partial_value
+    for hop in (1, 2, 4):
+        summed = summed + lax.ppermute(summed, "sp", [(dev, dev ^ hop) for dev in range(8)])
     own_read = summed.reshape(head_width).astype(jnp.bfloat16)
     reading = lax.all_gather(own_read, "tp", axis=0, tiled=True)
     return (key_cache, value_cache, reading)

time: 65.7 us -> 60.3 us (0.918)
  blocking collectives: 44 us -> 26.9 us
  waiting for transfers between devices: 0.01 us -> 11.6 us
    psum x1 -> x0, blocking collectives: 17.1 us -> none  [shards(): summed = lax.psum(partial_value, 'sp')]
    ppermute x0 -> x3, waiting for transfers between devices: none -> 11.6 us  [shards(): lax.ppermute(summed, 'sp', [(dev, dev ^ hop) for dev in range(8)])]
  transfers between devices with their start and end apart: 1 -> 4, of which waited for: 0 -> 3; matrix products, arithmetic and copies ran while one was open for 9% -> 10% of each run, Pallas kernels for 0% -> 0%
where the time goes in v1:
time: 60.3 us; the launch traced here: 60 us
  blocking collectives  26.9 us (45%)
  waiting for transfers between devices  11.6 us (19%)
  starting transfers between devices  7.32 us (12%)
  other arithmetic  5.62 us (9%)
  local copies, waits for them, and re-layouts  3.98 us (7%)
  matrix products  2.36 us (4%)
  between operations  2.16 us (4%)
    unnamed x1, blocking collectives  21.8 us
    ppermute x3, waiting for transfers between devices, shards(): lax.ppermute(summed, 'sp', [(dev, dev ^ hop) for dev in range(8)])  11.6 us
    all_to_all x1, starting transfers between devices, shards(): lax.all_to_all(outgoing, 'sp', split_axis=1, concat_axis=2, tiled=True)  7.31 us
    all_gather x1, blocking collectives, shards(): reading = lax.all_gather(own_read, 'tp', axis=0, tiled=True)  5.06 us
    another operation x2, other arithmetic  2.71 us
    reduce_sum x2, other arithmetic, norm_rows(): jnp.mean(wide_rows * wide_rows, axis=-1, keepdims=True) + 1e-06  2.34 us
    unnamed x21, local copies, waits for them, and re-layouts  1.43 us
    dot_general x1, matrix products, shards(): jnp.dot(normed, w_value, preferred_element_type=jnp.float32)  1.3 us
  transfers between devices with their start and end apart: 4, of which 3 were waited for; matrix products, arithmetic and copies ran while one was open for 10% of the time, Pallas kernels for 0%

profile of v1, /device:TPU:0, one launch (start us, length us, event | category | flops | bytes accessed | tf_op | source)
XLA Modules:
  0.0 60.0 jit_solution(8454295339224934806)
XLA Ops:
  0.6 0.0 copy-start
  0.7 1.7 %fusion = f32[288]{0:T(512)S(1)} fusion(bf16[288,2048]{1,0:T(8,128)(2,1)} %param.7), kind=kLoop, calls=%fused_computation.2 | loop fusion | flops 1769184 | bytes 1180800 | tf_op jit(solution)/shard_map/reduce_sum | solution.py:11
  2.4 0.2 copy-done.1
  2.6 1.3 %convolution_convert_fusion = bf16[288,256]{1,0:T(8,128)(2,1)S(1)} fusion(bf16[2048,256]{1,0:T(8,128)(2,1)S(1)} %copy-done, bf16[288,2048]{1,0:T(8,128)(2,1)S(1)} %copy-done.1, f32[2048]{0:T(1024)} %param.9, f32[288]{0:T(512)S(1)} %add_rsqrt_fusion), kind=kOutput, calls=%fused_computation.5 | convolution fusion | flops 304422912 | bytes 2385024 | tf_op jit(solution)/shard_map/dot_general | solution.py:24
  3.9 0.5 convolution_convert_fusion.1
  4.5 0.0 copy-start.3
  4.6 0.0 copy-start.7
  4.6 1.0 %copy.17 = bf16[2,8,1,36,256]{4,0,3,2,1:T(2,128)(2,1)} copy(bf16[2,8,1,36,256]{4,3,1,2,0:T(8,128)(2,1)S(1)} %pad_maximum_fusion) | data formatting | bytes 589824 | tf_op jit(solution)/shard_map/stack | solution.py:25
  5.6 7.3 %all-to-all-start = ((bf16[2,8,1,36,256]{4,0,3,2,1:T(2,128)(2,1)}), bf16[2,8,1,36,256]{4,0,3,2,1:T(2,128)(2,1)S(1)}, u32[]{:S(2)}, u32[]{:S(2)}) async-start(bf16[2,8,1,36,256]{4,0,3,2,1:T(2,128)(2,1)} %copy.17), calls=%async_computation | async-start | bytes 589824 | tf_op jit(solution)/shard_map/all_to_all | solution.py:26
  13.0 0.6 %fusion.11 = f32[]{:T(128)} fusion(bf16[2048]{0:T(1024)(128)(2,1)S(1)} %copy-done.3), kind=kLoop, calls=%fused_computation.20 | loop fusion | flops 6143 | bytes 4100 | tf_op jit(solution)/shard_map/reduce_sum | solution.py:11
  14.3 0.2 fusion.21
  14.5 0.1 fusion.8
  14.7 0.6 %dynamic-slice = u32[1]{0:T(128)} dynamic-slice(u32[32]{0:T(128)S(1)} %copy-done.7, u32[]{:T(128)S(6)} %add.60), dynamic_slice_sizes={1} | dynamic-slice | bytes 12
  16.0 0.1 fusion.19
  16.1 0.1 negate_dynamic-update-slice_fusion
  16.2 21.8 %all-reduce.1 = f32[16]{0:T(128)S(1)} all-reduce(f32[16]{0:T(128)S(1)} %negate_dynamic-update-slice_fusion), channel_id=2, replica_groups=mesh['sp'=8,'tp'=4] {'sp'}, use_global_device_ids=true, to_apply=%add.1 | all-reduce | flops 16 | bytes 128
  38.1 2.5 %reduce-window.6 = f32[2,3,128]{2,1,0:T(4,128)S(1)} reduce-window(f32[2,3,128]{2,1,0:T(4,128)S(1)} %reshape.81, f32[]{:T(128)} %constant.20.clone.1), window={size=1x1x128 pad=0_0x0_0x0_127}, to_apply=%region_2.3 | reduce-window | flops 97536 | bytes 6148 | tf_op jit(solution)/shard_map/reduce-window
  40.6 0.1 slice_reduce_fusion
  40.7 0.2 reduce-window.9
  40.9 0.1 slice.21
  40.9 0.1 add_bitcast_fusion
  41.0 0.1 reshape.84
  41.1 0.1 select_reduce_fusion
  41.2 0.1 exponential_bitcast_fusion
  41.3 0.1 fusion.5
  41.4 3.6 %collective-permute-done = f32[2,128]{1,0:T(2,128)S(1)} collective-permute-done((f32[2,128]{1,0:T(2,128)S(1)}, f32[2,128]{1,0:T(2,128)S(1)}, u32[]{:S(2)}, u32[]{:S(2)}) %collective-permute-start) | collective-permute-done | bytes 1056 | tf_op jit(solution)/shard_map/ppermute | solution.py:50
  45.0 3.6 %collective-permute-done.1 = f32[2,128]{1,0:T(2,128)S(1)} collective-permute-done((f32[2,128]{1,0:T(2,128)S(1)}, f32[2,128]{1,0:T(2,128)S(1)}, u32[]{:S(2)}, u32[]{:S(2)}) %collective-permute-start.1) | collective-permute-done | bytes 1056 | tf_op jit(solution)/shard_map/ppermute | solution.py:50
  48.6 4.5 %collective-permute-done.2 = f32[2,128]{1,0:T(2,128)S(1)} collective-permute-done((f32[2,128]{1,0:T(2,128)S(1)}, f32[2,128]{1,0:T(2,128)S(1)}, u32[]{:S(2)}, u32[]{:S(2)}) %collective-permute-start.2) | collective-permute-done | bytes 1056 | tf_op jit(solution)/shard_map/ppermute | solution.py:50
  53.1 5.1 %all-gather.1 = bf16[4,1,256]{2,1,0:T(2,128)(2,1)S(1)} all-gather(bf16[1,1,256]{2,1,0:T(2,128)(2,1)S(1)} %reshape.88), channel_id=1, replica_groups=mesh['sp'=8,'tp'=4] {'tp'}, dimensions={0}, use_global_device_ids=true | all-gather | bytes 2560 | tf_op jit(solution)/shard_map/all_gather | solution.py:52
  58.2 0.6 copy.31
  58.7 0.4 fusion.20
  59.2 0.8 %copy_bitcast_fusion = (bf16[1,8,36,256]{3,1,2,0:T(8,128)(2,1)}, bf16[1,8,36,256]{3,1,2,0:T(8,128)(2,1)}) fusion(bf16[1,8,1,36,256]{4,0,3,2,1:T(2,128)(2,1)S(1)} %get-tuple-element.11, bf16[1,8,1,36,256]{4,0,3,2,1:T(2,128)(2,1)S(1)} %get-tuple-element.12), kind=kLoop, calls=%fused_computation.14 | loop fusion | bytes 589824 | tf_op jit(solution)/shard_map/squeeze | solution.py:28
  (34 shorter events, 0.3 us)
Async XLA Ops:
  0.6 1.8 %copy-start = (bf16[2048,256]{1,0:T(8,128)(2,1)S(1)}, bf16[2048,256]{1,0:T(8,128)(2,1)}, u32[]{:S(2)}) copy-start(bf16[2048,256]{1,0:T(8,128)(2,1)} %param.11) | copy-start | bytes 3145732
  0.6 1.9 %copy-start.1 = (bf16[288,2048]{1,0:T(8,128)(2,1)S(1)}, bf16[288,2048]{1,0:T(8,128)(2,1)}, u32[]{:S(2)}) copy-start(bf16[288,2048]{1,0:T(8,128)(2,1)} %param.7) | copy-start | bytes 3538948
  2.6 1.3 %copy-start.5 = (f32[2048]{0:T(1024)S(1)}, f32[2048]{0:T(1024)}, u32[]{:S(2)}) copy-start(f32[2048]{0:T(1024)} %param.9) | copy-start | bytes 24580
  2.6 1.3 %copy-start.6 = (bf16[2048,256]{1,0:T(8,128)(2,1)S(1)}, bf16[2048,256]{1,0:T(8,128)(2,1)}, u32[]{:S(2)}) copy-start(bf16[2048,256]{1,0:T(8,128)(2,1)} %param.10) | copy-start | bytes 3145732
  4.5 8.5 %copy-start.3 = (bf16[2048]{0:T(1024)(128)(2,1)S(1)}, bf16[2048]{0:T(1024)(128)(2,1)}, u32[]{:S(2)}) copy-start(bf16[2048]{0:T(1024)(128)(2,1)} %param.8) | copy-start | bytes 12292
  4.5 9.8 %copy-start.2 = (bf16[2048,256]{1,0:T(8,128)(2,1)S(1)}, bf16[2048,256]{1,0:T(8,128)(2,1)}, u32[]{:S(2)}) copy-start(bf16[2048,256]{1,0:T(8,128)(2,1)} %param.12) | copy-start | bytes 3145732
  4.6 10.1 %copy-start.7 = (u32[32]{0:T(128)S(1)}, u32[32]{0:T(128)}, u32[]{:S(2)}) copy-start(u32[32]{0:T(128)} %constant.31) | copy-start | bytes 388
  4.6 11.3 %copy-start.4 = (f32[288,2]{0,1:T(2,128)S(1)}, f32[288,2]{0,1:T(2,128)}, u32[]{:S(2)}) copy-start(f32[288,2]{0,1:T(2,128)} %param.13) | copy-start | bytes 6916
  5.6 53.1 %all-to-all-start = ((bf16[2,8,1,36,256]{4,0,3,2,1:T(2,128)(2,1)}), bf16[2,8,1,36,256]{4,0,3,2,1:T(2,128)(2,1)S(1)}, u32[]{:S(2)}, u32[]{:S(2)}) async-start(bf16[2,8,1,36,256]{4,0,3,2,1:T(2,128)(2,1)} %copy.17), calls=%async_computation | async-start | bytes 589824 | tf_op jit(solution)/shard_map/all_to_all | solution.py:26
  41.4 3.6 %collective-permute-start = (f32[2,128]{1,0:T(2,128)S(1)}, f32[2,128]{1,0:T(2,128)S(1)}, u32[]{:S(2)}, u32[]{:S(2)}) collective-permute-start(f32[2,128]{1,0:T(2,128)S(1)} %bitcast.64), channel_id=1, source_target_pairs={{0,4},{4,0},{8,12},{12,8},{16,20},{20,16},{24,28},{28,24},{1,5},{5... | collective-permute-start | bytes 3080 | tf_op jit(solution)/shard_map/ppermute | solution.py:50
  45.0 3.6 %collective-permute-start.1 = (f32[2,128]{1,0:T(2,128)S(1)}, f32[2,128]{1,0:T(2,128)S(1)}, u32[]{:S(2)}, u32[]{:S(2)}) collective-permute-start(f32[2,128]{1,0:T(2,128)S(1)} %add.57), channel_id=1, source_target_pairs={{0,8},{4,12},{8,0},{12,4},{16,24},{20,28},{24,16},{28,20},{1,9},{5... | collective-permute-start | bytes 3080 | tf_op jit(solution)/shard_map/ppermute | solution.py:50
  48.6 4.5 %collective-permute-start.2 = (f32[2,128]{1,0:T(2,128)S(1)}, f32[2,128]{1,0:T(2,128)S(1)}, u32[]{:S(2)}, u32[]{:S(2)}) collective-permute-start(f32[2,128]{1,0:T(2,128)S(1)} %add.58), channel_id=1, source_target_pairs={{0,16},{4,20},{8,24},{12,28},{16,0},{20,4},{24,8},{28,12},{1,17},{... | collective-permute-start | bytes 3080 | tf_op jit(solution)/shard_map/ppermute | solution.py:50
